TPU v7x, 512 devices: a whole 4x8x8 slice. The times are simulated.
512 devices in a mesh: fs: 64 (over z, y), tp: 8 (over x, core).
Axes of the slice: x: 4, y: 8, z: 8, core: 2. Of those that a mesh axis runs over, the one named last changes fastest.
Arguments:
- inputs: bfloat16 [32768, 2048], P('fs', 'tp'), may hold values from -6 to 6
- hidden_pre: bfloat16 [32768, 4096], P('fs', 'tp'), may hold values from -6 to 6
- norm_input: bfloat16 [32768, 2048], P('fs', 'tp'), may hold values from -48 to 48, as said below
- out_gain: float32 [2048], P('tp'), may hold values from 0.1 to 1.9
- w_up: bfloat16 [2048, 4096], P('tp', 'fs'), may hold values from -0.125 to 0.125
- w_down: bfloat16 [4096, 2048], P('tp', 'fs'), may hold values from -0.09375 to 0.09375
- cotangent: bfloat16 [32768, 2048], P('fs', 'tp'), may hold values from -16 to 16
Outputs:
- grad_input: bfloat16 [32768, 2048], P('fs', 'tp')
- grad_up: float32 [2048, 4096], P('tp', 'fs')
- grad_gain: float32 [2048], P('tp')
Inputs may be any that keep to these rules, and one draw needn't show every extreme that they name: `norm_input`: each token's features are scaled by a factor of that token, and each block of 2048 / 8 features by a factor of that block.
All inputs are finite; a program needn't handle non-finite values.
Results may differ from a plain program's by a relative error of at most 0.0058.
Values may be sent and summed in bfloat16 or wider, within the bound.
No kernel may reach another device: no remote copies, remote signals or barrier semaphores. Data moves between devices by JAX's collectives and lax.ppermute only.
A program may use at most 64 MiB of HBM per device.

v0:
```python
import jax
import jax.numpy as jnp
from jax import lax
from jax.sharding import Mesh
from jax.sharding import PartitionSpec as P

FS = ("fs_0", "fs_1")
norm_eps = 1e-06


def from_everyone(value, axis):
    devices = lax.axis_size(axis)
    return lax.all_to_all(
        jnp.broadcast_to(value[None], (devices, *value.shape)), axis, 0, 0, tiled=True
    )


def taken_together(value, axis):
    everything = from_everyone(value, axis)
    return jnp.sum(everything, axis=0)


def in_one(arrays, axis):
    ends = [0]
    for a in arrays:
        ends.append(ends[-1] + a.size)
    total = taken_together(jnp.concatenate([a.ravel() for a in arrays]), axis)
    return tuple((total[b:e].reshape(a.shape) for a, b, e in zip(arrays, ends, ends[1:])))


def one_axis_at_a_time(value, axes):
    for axis in axes:
        value = lax.psum(value, axis)
    return value


def joined_along(parts, dim):
    parts = jnp.moveaxis(parts, 0, dim)
    dims = parts.shape
    return parts.reshape(*dims[:dim], dims[dim] * dims[dim + 1], *dims[dim + 2 :])


def gather_directly(value, axis, dim):
    parts = from_everyone(value, axis)
    return joined_along(parts, dim)


def stacked_from(value, axes, order):
    parts = value[None]
    for k in order:
        parts = lax.all_gather(parts, axes[k], axis=0, tiled=True)
    block = [lax.axis_size(axes[k]) for k in reversed(order)]
    parts = parts.reshape(*block, *value.shape)
    turned = sorted(range(len(order)), key=lambda place: order[len(order) - 1 - place])
    return parts.transpose(*turned, *range(len(order), parts.ndim)).reshape(-1, *value.shape)


def gather_axes(value, axes, order, dim):
    return joined_along(stacked_from(value, axes, order), dim)


def summed_rows(value, axes, dim):
    for axis in axes:
        value = lax.psum_scatter(value, axis, scatter_dimension=dim, tiled=True)
    return value


def on_device(inputs, hidden_pre, norm_input, out_gain, w_up, w_down, cotangent):
    tok_rows = inputs.shape[0]
    width = inputs.shape[1] * lax.axis_size("tp")
    scaled = (tok_rows * lax.axis_size(FS)) ** (-0.5)
    normed = norm_input.astype(jnp.float32)
    upstream = cotangent.astype(jnp.float32)
    weighted = upstream * out_gain
    square_sum, cross_sum = in_one(
        (jnp.sum(normed * normed, axis=1), jnp.sum(weighted * normed, axis=1)), "tp"
    )
    inv_rms = lax.rsqrt(square_sum / width + norm_eps)[:, None]
    cross_mean = (cross_sum / width)[:, None]
    d_out = (weighted * inv_rms - normed * inv_rms * inv_rms * inv_rms * cross_mean).astype(
        jnp.bfloat16
    )
    grad_gain = one_axis_at_a_time(jnp.sum(upstream * normed * inv_rms, axis=0) * scaled, FS)
    out_full = gather_directly(d_out, "tp", 1)
    columns = out_full
    d_act = lax.dot_general(
        columns,
        gather_axes(w_down, FS, (0, 1), 1),
        (((1,), (1,)), ((), ())),
        preferred_element_type=jnp.float32,
    )
    d_pre = (d_act * 2.0 * jax.nn.relu(hidden_pre.astype(jnp.float32))).astype(jnp.bfloat16)
    hidden_full = lax.all_gather(d_pre, "tp", axis=1, tiled=True)
    columns = hidden_full
    grad_input = lax.dot_general(
        columns,
        lax.all_gather(w_up, FS, axis=1, tiled=True),
        (((1,), (1,)), ((), ())),
        preferred_element_type=jnp.float32,
    ).astype(jnp.bfloat16)
    whole_term = (
        lax.dot_general(
            hidden_full, inputs, (((0,), (0,)), ((), ())), preferred_element_type=jnp.float32
        )
        * scaled
    )
    grad_up = summed_rows(whole_term, FS, 0).T
    return (grad_input, grad_up, grad_gain)


def solution(mesh):
    torus = Mesh(mesh.devices.reshape(8, 8, mesh.shape["tp"]), ("fs_0", "fs_1", "tp"))
    in_specs = (
        P(FS, "tp"),
        P(FS, "tp"),
        P(FS, "tp"),
        P("tp"),
        P("tp", FS),
        P("tp", FS),
        P(FS, "tp"),
    )
    out_specs = (P(FS, "tp"), P("tp", FS), P("tp"))
    return jax.shard_map(
        on_device, mesh=torus, in_specs=in_specs, out_specs=out_specs, check_vma=False
    )
```

profile of v0, /device:TPU:6, one launch (start us, length us, event | category | flops | bytes accessed | tf_op | source)
XLA Modules:
  0.0 246.0 jit_solution(17596367826111091204)
XLA Ops:
  8.0 0.0 copy-start
  8.0 0.0 all-gather.5.cloned.1.call-start
  8.1 31.5 %all-gather = bf16[4096,32]{0,1:T(8,128)(2,1)S(1)} all-gather(bf16[512,32]{0,1:T(8,128)(2,1)} %param.12), channel_id=2, replica_groups=mesh['fs_0'=8,'fs_1'=8,'tp'=8] {'fs_0'}, dimensions={0}, use_global_device_ids=true | all-gather | bytes 294912 | tf_op jit(solution)/shard_map/all_gather | solution.py:51
  39.5 0.8 copy.27
  40.3 0.0 all-gather.5.cloned.1.call-update
  40.4 1.3 fusion.5
  41.7 8.0 %all_to_all.11 = f32[8,1,1024]{2,1,0:T(1,128)S(1)} all-to-all(f32[8,1,1024]{2,1,0:T(1,128)S(1)} %broadcast_in_dim.6), channel_id=1, replica_groups=mesh['fs_0'=8,'fs_1'=8,'tp'=8] {'tp'}, dimensions={0} | all-to-all | bytes 65536 | tf_op jit(solution)/shard_map/all_to_all | solution.py:13
  49.7 1.3 fusion.11
  51.0 0.1 copy.20
  51.1 1.5 broadcast_in_dim.7
  52.6 5.6 %all-to-all-start.1 = ((bf16[8,512,256]{1,2,0:T(8,128)(2,1)}), bf16[8,512,256]{1,2,0:T(8,128)(2,1)S(1)}, u32[]{:S(2)}, u32[]{:S(2)}) async-start(bf16[8,512,256]{1,2,0:T(8,128)(2,1)} %broadcast_in_dim.7), calls=%async_computation.1 | async-start | bytes 4194304 | tf_op jit(solution)/shard_map/all_to_all | solution.py:13
  58.2 0.0 all-gather.7.cloned.1.call-start
  58.2 24.0 %all-gather.5.cloned.1.call-done = bf16[64,512,32]{1,0,2:T(8,128)(2,1)} async-done(((bf16[8,512,32]{1,0,2:T(8,128)(2,1)}), bf16[64,512,32]{1,0,2:T(8,128)(2,1)}) %all-gather.5.cloned.1.call-update) | async-done | bytes 2097168 | tf_op jit(solution)/shard_map/all_gather | solution.py:51
  82.2 4.2 %copy.22 = bf16[8,8,512,32]{2,3,1,0:T(8,128)(2,1)} copy(bf16[8,8,512,32]{2,0,1,3:T(8,128)(2,1)} %bitcast.22) | data formatting | bytes 4194304 | tf_op jit(solution)/shard_map/transpose | solution.py:55
  86.4 0.0 all-to-all-done.1
  86.4 0.0 copy-done.1
  86.4 3.7 %fusion.1 = bf16[512,512]{1,0:T(8,128)(2,1)} fusion(bf16[512,2048]{0,1:T(8,128)(2,1)S(1)} %bitcast.23, bf16[512,2048]{0,1:T(8,128)(2,1)} %bitcast.24, bf16[512,512]{1,0:T(8,128)(2,1)S(1)} %copy-done.1), kind=kOutput, calls=%fused_computation.3 | convolution fusion | flops 1075052544 | bytes 5242880 | tf_op jit(solution)/shard_map/dot_general | solution.py:86
  90.1 0.0 all-gather.7.cloned.1.call-update
  90.1 0.0 reduce-scatter.3.cloned.1.call-start
  90.2 34.4 %all-gather.7.cloned.1.call-done = bf16[512,4096]{1,0:T(8,128)(2,1)} async-done(((bf16[512,512]{1,0:T(8,128)(2,1)}), bf16[512,4096]{1,0:T(8,128)(2,1)}) %all-gather.7.cloned.1.call-update) | async-done | bytes 4194320 | tf_op jit(solution)/shard_map/all_gather | solution.py:93
  124.6 0.0 copy-done
  124.6 5.4 %convolution_multiply_fusion = f32[4096,256]{1,0:T(8,128)} fusion(bf16[512,4096]{1,0:T(8,128)(2,1)} %all-gather.7.cloned.1.call-done, bf16[512,256]{1,0:T(8,128)(2,1)S(1)} %copy-done), kind=kOutput, calls=%fused_computation | convolution fusion | flops 1074790400 | bytes 8650752 | tf_op jit(solution)/shard_map/dot_general | solution.py:102
  130.0 0.0 reduce-scatter.3.cloned.1.call-update
  130.0 0.0 all-gather.9.cloned.1.call-start
  130.1 0.5 all-gather.9.cloned.1.call-update
  130.6 0.0 reduce-scatter.5.cloned.1.call-start
  130.7 61.3 %reduce-scatter.3.cloned.1.call-done = f32[512,256]{1,0:T(8,128)} async-done(((f32[4096,256]{1,0:T(8,128)}), f32[512,256]{1,0:T(8,128)}) %reduce-scatter.3.cloned.1.call-update) | async-done | bytes 524304 | tf_op jit(solution)/shard_map/reduce_scatter | solution.py:64
  192.0 0.0 reduce-scatter.5.cloned.1.call-update
  192.0 15.4 %psum.14 = f32[256]{0:T(256)S(1)} all-reduce(f32[256]{0:T(256)S(1)} %broadcast_multiply_fusion), channel_id=1, replica_groups=mesh['fs_0'=8,'fs_1'=8,'tp'=8] {'fs_0'}, use_global_device_ids=true, to_apply=%region_6.7 | all-reduce | flops 256 | bytes 2048 | tf_op jit(solution)/shard_map/psum | solution.py:33
  207.4 17.6 %psum.15 = f32[256]{0:T(256)} all-reduce(f32[256]{0:T(256)S(1)} %psum.14), channel_id=1, replica_groups=mesh['fs_0'=8,'fs_1'=8,'tp'=8] {'fs_1'}, use_global_device_ids=true, to_apply=%region_7.8 | all-reduce | flops 256 | bytes 2048 | tf_op jit(solution)/shard_map/psum | solution.py:33
  225.1 9.0 %all-gather.9.cloned.1.call-done = bf16[256,4096]{0,1:T(8,128)(2,1)} async-done(((bf16[256,64]{0,1:T(8,128)(2,1)}), bf16[256,4096]{0,1:T(8,128)(2,1)}) %all-gather.9.cloned.1.call-update) | async-done | bytes 2097168 | tf_op jit(solution)/shard_map/all_gather | solution.py:97
  234.1 4.8 %convolution_convert_fusion = bf16[512,256]{1,0:T(8,128)(2,1)} fusion(bf16[512,4096]{1,0:T(8,128)(2,1)} %all-gather.7.cloned.1.call-done, bf16[256,4096]{0,1:T(8,128)(2,1)} %all-gather.9.cloned.1.call-done), kind=kOutput, calls=%fused_computation.4 | convolution fusion | flops 1073872896 | bytes 6553600 | tf_op jit(solution)/shard_map/dot_general | solution.py:95
  (7 shorter events, 0.1 us)
Async XLA Ops:
  8.0 116.6 %copy-start = (bf16[512,256]{1,0:T(8,128)(2,1)S(1)}, bf16[512,256]{1,0:T(8,128)(2,1)}, u32[]{:S(2)}) copy-start(bf16[512,256]{1,0:T(8,128)(2,1)} %param.7) | copy-start | bytes 786436
  8.0 74.2 %all-gather.5.cloned.1.call-start = ((), (), s32[]{:S(2)}) async-start(), calls=%async_computation.4 | async-start | bytes 2359296 | tf_op jit(solution)/shard_map/all_gather | solution.py:51
  52.6 33.8 %all-to-all-start.1 = ((bf16[8,512,256]{1,2,0:T(8,128)(2,1)}), bf16[8,512,256]{1,2,0:T(8,128)(2,1)S(1)}, u32[]{:S(2)}, u32[]{:S(2)}) async-start(bf16[8,512,256]{1,2,0:T(8,128)(2,1)} %broadcast_in_dim.7), calls=%async_computation.1 | async-start | bytes 4194304 | tf_op jit(solution)/shard_map/all_to_all | solution.py:13
  58.2 66.3 %all-gather.7.cloned.1.call-start = ((), (), s32[]{:S(2)}) async-start(), calls=%async_computation.5 | async-start | bytes 4718592 | tf_op jit(solution)/shard_map/all_gather | solution.py:93
  82.2 4.2 %copy-start.1 = (bf16[512,512]{1,0:T(8,128)(2,1)S(1)}, bf16[512,512]{1,0:T(8,128)(2,1)}, u32[]{:S(2)}) copy-start(bf16[512,512]{1,0:T(8,128)(2,1)} %param.8) | copy-start | bytes 1572868
  90.1 101.9 %reduce-scatter.3.cloned.1.call-start = ((), (), s32[]{:S(2)}) async-start(), calls=%async_computation.7 | async-start | bytes 4718592 | tf_op jit(solution)/shard_map/reduce_scatter | solution.py:64
  130.0 104.0 %all-gather.9.cloned.1.call-start = ((), (), s32[]{:S(2)}) async-start(), calls=%async_computation.6 | async-start | bytes 2129920 | tf_op jit(solution)/shard_map/all_gather | solution.py:97
  130.6 108.3 %reduce-scatter.5.cloned.1.call-start = ((), (), s32[]{:S(2)}) async-start(), calls=%async_computation.8 | async-start | bytes 589824 | tf_op jit(solution)/shard_map/reduce_scatter | solution.py:64
Sparse Core Ops, SparseCore 0:
  40.5 41.7 all-gather.4
  90.2 34.2 all-gather.6
  130.1 61.7 reduce-scatter.2
  195.2 38.8 reduce-scatter.4
Sparse Core Ops, SparseCore 1:
  133.6 100.4 all-gather.8
where the time goes:
time: 246 us
  waiting for transfers between devices  129 us (52%)
  blocking collectives  72.5 us (29%)
  between operations  15.3 us (6%)
  matrix products  13.9 us (6%)
  local copies, waits for them, and re-layouts  6.63 us (3%)
  starting transfers between devices  5.77 us (2%)
  other arithmetic  2.63 us (1%)
    reduce_scatter x2, waiting for transfers between devices, summed_rows(): value = lax.psum_scatter(value, axis, scatter_dimension=dim, tiled=True)  61.3 us
    all_gather x1, waiting for transfers between devices, on_device(): hidden_full = lax.all_gather(d_pre, 'tp', axis=1, tiled=True)  34.4 us
    psum x2, blocking collectives, one_axis_at_a_time(): value = lax.psum(value, axis)  33.1 us
    all_gather x1, blocking collectives, stacked_from(): parts = lax.all_gather(parts, axes[k], axis=0, tiled=True)  31.5 us
    all_gather x1, waiting for transfers between devices, stacked_from(): parts = lax.all_gather(parts, axes[k], axis=0, tiled=True)  24 us
    all_gather x1, waiting for transfers between devices, on_device(): lax.all_gather(w_up, FS, axis=1, tiled=True)  9 us
    all_to_all x1, blocking collectives, from_everyone(): lax.all_to_all(jnp.broadcast_to(value[None], (devices, *value.shape)), ax...  7.95 us
    all_to_all x1, starting transfers between devices, from_everyone(): lax.all_to_all(jnp.broadcast_to(value[None], (devices, *value.shape)), ax...  5.61 us
  transfers between devices with their start and end apart: 6, of which 4 were waited for; matrix products, arithmetic and copies ran while one was open for 5% of the time, Pallas kernels for 0%

commit v1 on v0

--- a/solution.py
+++ b/solution.py
@@ -1,3 +1,4 @@
+import functools
 import jax
 import jax.numpy as jnp
 from jax import lax
@@ -6,6 +7,16 @@
 
 FS = ("fs_0", "fs_1")
 norm_eps = 1e-06
+
+
+def set_keys_on_mesh(x0, in_dim):
+    state_now = lax.psum(1, "tp")
+    new = jnp.stack([x0] * state_now)
+    found_now = lax.all_to_all(new, "tp", 0, 0)
+    return jnp.concatenate(found_now, in_dim)
+
+
+wait_indices = functools.partial(set_keys_on_mesh, in_dim=1)
 
 
 def from_everyone(value, axis):
@@ -90,7 +101,7 @@
         preferred_element_type=jnp.float32,
     )
     d_pre = (d_act * 2.0 * jax.nn.relu(hidden_pre.astype(jnp.float32))).astype(jnp.bfloat16)
-    hidden_full = lax.all_gather(d_pre, "tp", axis=1, tiled=True)
+    hidden_full = wait_indices(d_pre)
     columns = hidden_full
     grad_input = lax.dot_general(
         columns,

time: 246 us -> 260 us (1.057)
  blocking collectives: 72.5 us -> 125 us
  waiting for transfers between devices: 129 us -> 90.9 us
  matrix products: 13.9 us -> 11 us
    all_to_all x0 -> x1, blocking collectives: none -> 52.2 us  [set_keys_on_mesh(): found_now = lax.all_to_all(new, 'tp', 0, 0)]
    all_gather x1 -> x0, waiting for transfers between devices: 34.4 us -> none  [on_device(): hidden_full = lax.all_gather(d_pre, 'tp', axis=1, tiled=True)]
    reduce_scatter x2, waiting for transfers between devices: 61.3 us -> 57.9 us  [summed_rows(): value = lax.psum_scatter(value, axis, scatter_dimension=dim, tiled=True)]
  transfers between devices with their start and end apart: 6 -> 5, of which waited for: 4 -> 3; matrix products, arithmetic and copies ran while one was open for 5% -> 5% of each run, Pallas kernels for 0% -> 0%
where the time goes in v1:
time: 260 us; the launch traced here: 259 us
  blocking collectives  125 us (48%)
  waiting for transfers between devices  90.9 us (35%)
  between operations  15.3 us (6%)
  matrix products  11 us (4%)
  local copies, waits for them, and re-layouts  9.06 us (3%)
  starting transfers between devices  5.73 us (2%)
  other arithmetic  2.63 us (1%)
    reduce_scatter x2, waiting for transfers between devices, summed_rows(): value = lax.psum_scatter(value, axis, scatter_dimension=dim, tiled=True)  57.9 us
    all_to_all x1, blocking collectives, set_keys_on_mesh(): found_now = lax.all_to_all(new, 'tp', 0, 0)  52.2 us
    psum x2, blocking collectives, one_axis_at_a_time(): value = lax.psum(value, axis)  33.1 us
    all_gather x1, blocking collectives, stacked_from(): parts = lax.all_gather(parts, axes[k], axis=0, tiled=True)  31.5 us
    all_gather x1, waiting for transfers between devices, stacked_from(): parts = lax.all_gather(parts, axes[k], axis=0, tiled=True)  24 us
    all_gather x1, waiting for transfers between devices, on_device(): lax.all_gather(w_up, FS, axis=1, tiled=True)  8.42 us
    all_to_all x1, blocking collectives, from_everyone(): lax.all_to_all(jnp.broadcast_to(value[None], (devices, *value.shape)), ax...  7.95 us
    all_to_all x1, starting transfers between devices, from_everyone(): lax.all_to_all(jnp.broadcast_to(value[None], (devices, *value.shape)), ax...  5.61 us
  transfers between devices with their start and end apart: 5, of which 3 were waited for; matrix products, arithmetic and copies ran while one was open for 5% of the time, Pallas kernels for 0%

profile of v1, /device:TPU:6, one launch (start us, length us, event | category | flops | bytes accessed | tf_op | source)
XLA Modules:
  0.0 259.3 jit_solution(5526118361526320037)
XLA Ops:
  8.0 0.0 copy-start
  8.0 0.0 all-gather.4.cloned.1.call-start
  8.1 31.5 %all-gather = bf16[4096,32]{0,1:T(8,128)(2,1)S(1)} all-gather(bf16[512,32]{0,1:T(8,128)(2,1)} %param.12), channel_id=2, replica_groups=mesh['fs_0'=8,'fs_1'=8,'tp'=8] {'fs_0'}, dimensions={0}, use_global_device_ids=true | all-gather | bytes 294912 | tf_op jit(solution)/shard_map/all_gather | solution.py:62
  39.5 0.8 copy.32
  40.3 0.0 all-gather.4.cloned.1.call-update
  40.4 1.3 fusion.5
  41.7 8.0 %all_to_all.16 = f32[8,1,1024]{2,1,0:T(1,128)S(1)} all-to-all(f32[8,1,1024]{2,1,0:T(1,128)S(1)} %broadcast_in_dim.6), channel_id=1, replica_groups=mesh['fs_0'=8,'fs_1'=8,'tp'=8] {'tp'}, dimensions={0} | all-to-all | bytes 65536 | tf_op jit(solution)/shard_map/all_to_all | solution.py:24
  49.7 1.3 fusion.11
  51.0 0.1 copy.24
  51.1 1.5 broadcast_in_dim.7
  52.6 5.6 %all-to-all-start.1 = ((bf16[8,512,256]{1,2,0:T(8,128)(2,1)}), bf16[8,512,256]{1,2,0:T(8,128)(2,1)S(1)}, u32[]{:S(2)}, u32[]{:S(2)}) async-start(bf16[8,512,256]{1,2,0:T(8,128)(2,1)} %broadcast_in_dim.7), calls=%async_computation.1 | async-start | bytes 4194304 | tf_op jit(solution)/shard_map/all_to_all | solution.py:24
  58.2 0.0 reduce-scatter.3.cloned.1.call-start
  58.2 24.0 %all-gather.4.cloned.1.call-done = bf16[64,512,32]{1,0,2:T(8,128)(2,1)} async-done(((bf16[8,512,32]{1,0,2:T(8,128)(2,1)}), bf16[64,512,32]{1,0,2:T(8,128)(2,1)}) %all-gather.4.cloned.1.call-update) | async-done | bytes 2097168 | tf_op jit(solution)/shard_map/all_gather | solution.py:62
  82.2 4.1 %copy.26 = bf16[8,8,512,32]{2,3,1,0:T(8,128)(2,1)} copy(bf16[8,8,512,32]{2,0,1,3:T(8,128)(2,1)} %bitcast.27) | data formatting | bytes 4194304 | tf_op jit(solution)/shard_map/transpose | solution.py:66
  86.4 0.0 all-to-all-done.1
  86.4 0.0 copy-done.2
  86.4 2.9 %fusion.1 = bf16[512,512]{1,0:T(8,128)(2,1)S(1)} fusion(bf16[512,2048]{0,1:T(8,128)(2,1)S(1)} %bitcast.28, bf16[512,2048]{0,1:T(8,128)(2,1)} %bitcast.29, bf16[512,512]{1,0:T(8,128)(2,1)S(1)} %copy-done.2), kind=kOutput, calls=%fused_computation.3 | convolution fusion | flops 1075052544 | bytes 5242880 | tf_op jit(solution)/shard_map/dot_general | solution.py:97
  89.3 0.2 copy.27
  89.5 0.4 stack.2
  89.9 52.2 %all_to_all.17 = bf16[8,512,512]{1,2,0:T(8,128)(2,1)S(1)} all-to-all(bf16[8,512,512]{1,2,0:T(8,128)(2,1)S(1)} %stack.2), channel_id=1, replica_groups=mesh['fs_0'=8,'fs_1'=8,'tp'=8] {'tp'}, dimensions={0} | all-to-all | bytes 8388608 | tf_op jit(solution)/shard_map/all_to_all | solution.py:15
  142.1 1.9 copy-done.1
  144.0 3.2 %convolution_multiply_fusion = f32[4096,256]{1,0:T(8,128)} fusion(bf16[512,4096]{0,1:T(8,128)(2,1)S(1)} %bitcast.25, bf16[512,256]{1,0:T(8,128)(2,1)S(1)} %copy-done), kind=kOutput, calls=%fused_computation | convolution fusion | flops 1074790400 | bytes 8650752 | tf_op jit(solution)/shard_map/dot_general | solution.py:113
  147.2 0.0 reduce-scatter.3.cloned.1.call-update
  147.2 0.0 all-gather.6.cloned.1.call-start
  147.3 0.5 all-gather.6.cloned.1.call-update
  147.8 0.0 reduce-scatter.5.cloned.1.call-start
  147.9 57.9 %reduce-scatter.3.cloned.1.call-done = f32[512,256]{1,0:T(8,128)} async-done(((f32[4096,256]{1,0:T(8,128)}), f32[512,256]{1,0:T(8,128)}) %reduce-scatter.3.cloned.1.call-update) | async-done | bytes 524304 | tf_op jit(solution)/shard_map/reduce_scatter | solution.py:75
  205.8 0.0 reduce-scatter.5.cloned.1.call-update
  205.8 15.4 %psum.14 = f32[256]{0:T(256)S(1)} all-reduce(f32[256]{0:T(256)S(1)} %broadcast_multiply_fusion), channel_id=1, replica_groups=mesh['fs_0'=8,'fs_1'=8,'tp'=8] {'fs_0'}, use_global_device_ids=true, to_apply=%region_6.7 | all-reduce | flops 256 | bytes 2048 | tf_op jit(solution)/shard_map/psum | solution.py:44
  221.3 17.6 %psum.15 = f32[256]{0:T(256)} all-reduce(f32[256]{0:T(256)S(1)} %psum.14), channel_id=1, replica_groups=mesh['fs_0'=8,'fs_1'=8,'tp'=8] {'fs_1'}, use_global_device_ids=true, to_apply=%region_7.8 | all-reduce | flops 256 | bytes 2048 | tf_op jit(solution)/shard_map/psum | solution.py:44
  238.9 8.4 %all-gather.6.cloned.1.call-done = bf16[256,4096]{0,1:T(8,128)(2,1)} async-done(((bf16[256,64]{0,1:T(8,128)(2,1)}), bf16[256,4096]{0,1:T(8,128)(2,1)}) %all-gather.6.cloned.1.call-update) | async-done | bytes 2097168 | tf_op jit(solution)/shard_map/all_gather | solution.py:108
  247.3 4.9 %convolution_convert_fusion = bf16[512,256]{1,0:T(8,128)(2,1)} fusion(bf16[512,4096]{0,1:T(8,128)(2,1)} %bitcast.26, bf16[256,4096]{0,1:T(8,128)(2,1)} %all-gather.6.cloned.1.call-done), kind=kOutput, calls=%fused_computation.4 | convolution fusion | flops 1073872896 | bytes 6553600 | tf_op jit(solution)/shard_map/dot_general | solution.py:106
  (9 shorter events, 0.1 us)
Async XLA Ops:
  8.0 136.0 %copy-start = (bf16[512,256]{1,0:T(8,128)(2,1)S(1)}, bf16[512,256]{1,0:T(8,128)(2,1)}, u32[]{:S(2)}) copy-start(bf16[512,256]{1,0:T(8,128)(2,1)} %param.7) | copy-start | bytes 786436
  8.0 74.2 %all-gather.4.cloned.1.call-start = ((), (), s32[]{:S(2)}) async-start(), calls=%async_computation.5 | async-start | bytes 2359296 | tf_op jit(solution)/shard_map/all_gather | solution.py:62
  52.6 33.8 %all-to-all-start.1 = ((bf16[8,512,256]{1,2,0:T(8,128)(2,1)}), bf16[8,512,256]{1,2,0:T(8,128)(2,1)S(1)}, u32[]{:S(2)}, u32[]{:S(2)}) async-start(bf16[8,512,256]{1,2,0:T(8,128)(2,1)} %broadcast_in_dim.7), calls=%async_computation.1 | async-start | bytes 4194304 | tf_op jit(solution)/shard_map/all_to_all | solution.py:24
  58.2 147.6 %reduce-scatter.3.cloned.1.call-start = ((), (), s32[]{:S(2)}) async-start(), calls=%async_computation.7 | async-start | bytes 4718592 | tf_op jit(solution)/shard_map/reduce_scatter | solution.py:75
  82.2 4.1 %copy-start.2 = (bf16[512,512]{1,0:T(8,128)(2,1)S(1)}, bf16[512,512]{1,0:T(8,128)(2,1)}, u32[]{:S(2)}) copy-start(bf16[512,512]{1,0:T(8,128)(2,1)} %param.8) | copy-start | bytes 1572868
  142.1 1.9 copy-start.1
  147.2 100.1 %all-gather.6.cloned.1.call-start = ((), (), s32[]{:S(2)}) async-start(), calls=%async_computation.6 | async-start | bytes 2129920 | tf_op jit(solution)/shard_map/all_gather | solution.py:108
  147.8 104.4 %reduce-scatter.5.cloned.1.call-start = ((), (), s32[]{:S(2)}) async-start(), calls=%async_computation.8 | async-start | bytes 589824 | tf_op jit(solution)/shard_map/reduce_scatter | solution.py:75
Sparse Core Ops, SparseCore 0:
  40.5 41.7 all-gather.3
  147.4 58.3 reduce-scatter.2
  209.2 38.7 reduce-scatter.4
Sparse Core Ops, SparseCore 1:
  150.8 96.5 all-gather.5
